TPU v7x, 32 devices: a whole 2x2x4 slice. The times are simulated.
32 devices in a mesh: grp: 2 (over y), sp: 4 (over z), tp: 4 (over x, core).
Axes of the slice: x: 2, y: 2, z: 4, core: 2. Of those that a mesh axis runs over, the one named last changes fastest.
Arguments:
- queries: bfloat16 [4096, 1024], P(('grp', 'sp'), 'tp'), parts along dimension 0, may hold values from -5 to 9
- keys: bfloat16 [4096, 1024], P(('grp', 'sp'), 'tp'), parts along dimension 0, may hold values from -12 to 5
- values: bfloat16 [4096, 1024], P(('grp', 'sp'), 'tp'), parts along dimension 0, may hold values from -5 to 5
- residual: bfloat16 [4096, 2048], P(('grp', 'sp')), parts along dimension 0, may hold values from -6 to 6
- out_weight: bfloat16 [1024, 2048], P('tp'), may hold values from -0.1875 to 0.1875
- post_gain: float32 [2048], replicated, may hold values from 0.1 to 1.9
- gate_weight: bfloat16 [2048, 5120], P('sp', 'tp'), may hold values from -0.125 to 0.125
- up_weight: bfloat16 [2048, 5120], P('sp', 'tp'), may hold values from -0.125 to 0.125
- down_weight: bfloat16 [5120, 2048], P('tp', 'sp'), may hold values from -0.078125 to 0.078125
- ffn_pre_gain: float32 [2048], replicated, may hold values from 0.1 to 1.9
- ffn_post_gain: float32 [2048], replicated, may hold values from 0.1 to 1.9
Outputs:
- layer_out: bfloat16 [4096, 2048], P(('grp', 'sp', 'tp')), parts along dimension 0
There are 2 independent parts, one for each index of `grp`. A program takes and returns all parts, laid end to end along the dimension named above; an argument that names none is the same for every part. Nothing has to cross between parts.
All inputs are finite; a program needn't handle non-finite values.
Results may differ from a plain program's by a relative error of at most 0.014.
Values may be sent and summed in bfloat16 or wider, within the bound.
A program may use at most 64 MiB of HBM per device.

v0:
```python
import functools
import math

import jax
import jax.numpy as jnp
from jax import lax
from jax.experimental import pallas as pl
from jax.experimental.pallas import tpu as pltpu
from jax.sharding import PartitionSpec as P

HEAD_DIM = 64


norm_eps = 1e-06


def rms_scale(row_block, gain):
    mean_square = jnp.mean(row_block * row_block, axis=-1, keepdims=True)
    return row_block * lax.rsqrt(mean_square + norm_eps) * gain


def attention_block(q_ref, k_ref, v_ref, acc_ref, gone_ref, block_index, span, masked):
    rows = q_ref.shape[1]
    key_rows = pl.ds(pl.multiple_of(block_index * span, span), span)
    key_block = k_ref[key_rows, :]
    value_block = v_ref[key_rows, :]
    row_iota = lax.broadcasted_iota(jnp.int32, (span, span), 0)
    col_iota = lax.broadcasted_iota(jnp.int32, (span, span), 1)
    later = jnp.where(row_iota > col_iota, 1.0, 0.0).astype(jnp.bfloat16)
    lane_head = lax.broadcasted_iota(jnp.int32, acc_ref.shape, 1) // HEAD_DIM
    for head in range(q_ref.shape[0]):
        scores = lax.dot_general(
            q_ref[head], key_block, (((1,), (1,)), ((), ())), preferred_element_type=jnp.float32
        )
        soft = jnp.maximum(scores, 0.0) + jnp.log(1.0 + jnp.exp(-jnp.abs(scores)))
        expo = scores - soft
        if masked:
            strict = col_iota < row_iota
            soft = jnp.where(strict, soft, 0.0)
        tail = jnp.dot(soft.astype(jnp.bfloat16), later, preferred_element_type=jnp.float32)
        gone = gone_ref[head]
        wide = jnp.concatenate([gone] * (span // gone.shape[1]), axis=1)
        weights = jnp.exp(expo - (tail + wide))
        if masked:
            weights = jnp.where(strict, weights, 0.0)
        part = jnp.dot(
            weights.astype(jnp.bfloat16), value_block, preferred_element_type=jnp.float32
        )
        acc_ref[...] += jnp.where(lane_head == head, part, 0.0)
        total = tail[:, :1] + soft[:, :1]
        gone_ref[head] = gone + jnp.broadcast_to(total, gone.shape)


def attention_kernel(row_ref, q_ref, k_ref, v_ref, out_ref, acc_ref, gone_ref, *, span):
    diagonal = row_ref[0] // span + pl.program_id(1)
    acc_ref[...] = jnp.zeros_like(acc_ref)
    gone_ref[...] = jnp.zeros_like(gone_ref)
    attention_block(q_ref, k_ref, v_ref, acc_ref, gone_ref, diagonal, span, True)

    def turn(step, carry):
        attention_block(
            q_ref, k_ref, v_ref, acc_ref, gone_ref, diagonal - 1 - step, span, False
        )
        return carry

    lax.fori_loop(0, diagonal, turn, 0)
    out_ref[...] = acc_ref[...].astype(out_ref.dtype)


def stick_attention(queries, keys_values, first_row):
    tok_rows, width = queries.shape
    key_total = keys_values.shape[0]
    span = math.gcd(256, tok_rows)
    lanes = 128
    pack = lanes // HEAD_DIM
    column_groups = width // lanes
    lane_head = (jnp.arange(width) % lanes) // HEAD_DIM
    scaled = queries * jnp.asarray(1.0 / math.sqrt(HEAD_DIM), queries.dtype)
    split_queries = jnp.stack(
        [jnp.where(lane_head[None, :] == head, scaled, jnp.zeros_like(scaled)) for head in range(pack)]
    )
    grid_spec = pltpu.PrefetchScalarGridSpec(
        num_scalar_prefetch=1,
        grid=(column_groups, tok_rows // span),
        in_specs=[
            pl.BlockSpec((pack, span, lanes), lambda p, i, row: (0, i, p)),
            pl.BlockSpec((key_total, lanes), lambda p, i, row: (0, p)),
            pl.BlockSpec((key_total, lanes), lambda p, i, row: (0, column_groups + p)),
        ],
        out_specs=pl.BlockSpec((span, lanes), lambda p, i, row: (i, p)),
        scratch_shapes=[
            pltpu.VMEM((span, lanes), jnp.float32),
            pltpu.VMEM((pack, span, lanes), jnp.float32),
        ],
    )
    return pl.pallas_call(
        functools.partial(attention_kernel, span=span),
        grid_spec=grid_spec,
        out_shape=jax.ShapeDtypeStruct((tok_rows, width), jnp.bfloat16),
        compiler_params=pltpu.CompilerParams(vmem_limit_bytes=40 * 2**20),
        name="stick_attention",
    )(jnp.reshape(first_row, (1,)).astype(jnp.int32), split_queries, keys_values, keys_values)


def half_gather(weight, side):
    half = weight.shape[0] // 2
    mine = lax.dynamic_slice_in_dim(weight, side * half, half, 0)
    mine = lax.all_gather(mine, "sp", axis=0, tiled=True)
    other = lax.ppermute(mine, "grp", [(0, 1), (1, 0)])
    return mine, other


def per_device(
    queries,
    keys,
    values,
    residual,
    out_weight,
    post_gain,
    gate_weight,
    up_weight,
    down_weight,
    ffn_pre_gain,
    ffn_post_gain,
):
    tok_rows = queries.shape[0]
    tp_share = lax.axis_size("tp")
    part_rows = tok_rows // tp_share
    my_rows = lax.axis_index("tp") * part_rows
    side = lax.axis_index("grp")
    keys_values = lax.all_gather(jnp.concatenate([keys, values], axis=1), "sp", axis=0, tiled=True)
    gate_mine, gate_other = half_gather(gate_weight, side)
    up_mine, up_other = half_gather(up_weight, side)
    down_all = lax.all_gather(down_weight, "sp", axis=1, tiled=True)
    attended = stick_attention(queries, keys_values, lax.axis_index("sp") * tok_rows)
    mixed_sum = lax.psum(
        jnp.dot(attended, out_weight, preferred_element_type=jnp.float32).astype(jnp.bfloat16), "tp"
    ).astype(jnp.float32)
    first_all = residual.astype(jnp.float32) + rms_scale(mixed_sum, post_gain)
    ffn_in = rms_scale(first_all, ffn_pre_gain).astype(jnp.bfloat16)
    first_mine = lax.dynamic_slice_in_dim(first_all, my_rows, part_rows, 0)
    half = gate_weight.shape[0] // 2
    pieces = ffn_in.reshape(tok_rows, -1, 2, half)
    in_mine = lax.dynamic_index_in_dim(pieces, side, 2, False).reshape(tok_rows, -1)
    in_other = lax.dynamic_index_in_dim(pieces, 1 - side, 2, False).reshape(tok_rows, -1)
    gate_sum = jnp.dot(in_mine, gate_mine, preferred_element_type=jnp.float32) + jnp.dot(
        in_other, gate_other, preferred_element_type=jnp.float32
    )
    up_sum = jnp.dot(in_mine, up_mine, preferred_element_type=jnp.float32) + jnp.dot(
        in_other, up_other, preferred_element_type=jnp.float32
    )
    hidden = (jax.nn.silu(gate_sum) * up_sum).astype(jnp.bfloat16)
    ffn_terms = jnp.dot(
        hidden,
        down_all,
        preferred_element_type=jnp.float32,
    )
    ffn_out = lax.psum_scatter(
        ffn_terms.astype(jnp.bfloat16), "tp", scatter_dimension=0, tiled=True
    ).astype(jnp.float32)
    result = first_mine + 0.5 * rms_scale(ffn_out, ffn_post_gain)
    return result.astype(jnp.bfloat16)


def solution(mesh):
    in_specs = (
        P(("grp", "sp"), "tp"),
        P(("grp", "sp"), "tp"),
        P(("grp", "sp"), "tp"),
        P(("grp", "sp"), None),
        P("tp", None),
        P(),
        P("sp", "tp"),
        P("sp", "tp"),
        P("tp", "sp"),
        P(),
        P(),
    )
    out_specs = P(("grp", "sp", "tp"), None)
    return jax.shard_map(
        per_device, mesh=mesh, in_specs=in_specs, out_specs=out_specs, check_vma=False
    )
```

profile of v0, /device:TPU:0, one launch (start us, length us, event | category | flops | bytes accessed | tf_op | source)
XLA Modules:
  0.0 370.5 jit_solution(4822147923113536170)
XLA Ops:
  6.5 2.0 pad_maximum_fusion.1
  8.6 0.0 all-gather.5.cloned.1.call-update
  8.6 0.0 all-gather.7.cloned.1.call-start
  8.6 0.9 constant_dynamic-slice_fusion.2
  9.5 0.0 all-gather.7.cloned.1.call-update
  9.5 0.0 all-gather.9.cloned.1.call-start
  9.6 0.0 copy-done.7
  9.6 0.9 constant_dynamic-slice_fusion
  10.5 0.0 all-gather.9.cloned.1.call-update
  10.5 0.0 all-reduce.2.cloned.1.call-start
  10.7 0.0 copy-start.6
  10.7 0.1 pad_maximum_fusion.q_ref
  10.7 46.6 %all-gather.5.cloned.1.call-done.k_ref.v_ref = bf16[2048,512]{1,0:T(8,128)(2,1)} async-done(((bf16[512,512]{1,0:T(8,128)(2,1)}), bf16[2048,512]{1,0:T(8,128)(2,1)}) %all-gather.5.cloned.1.call-update) | async-done | bytes 2097168 | tf_op jit(solution)/shard_map/all_gather | solution.py:131
  57.3 1.6 copy-done.1
  58.9 5.0 %stick_attention.1 = bf16[512,256]{1,0:T(8,128)(2,1)S(1)} custom-call(s32[1]{0:T(128)} %bitcast.row_ref, bf16[2,512,256]{2,1,0:T(8,128)(2,1)S(1)} %pad_maximum_fusion.q_ref, bf16[2048,512]{1,0:T(8,128)(2,1)S(1)} %copy-done.1, bf16[2048,512]{1,0:T(8,128)(2,1)S(1)} %copy-done.1), custom_call_target="tpu_custom_call" | custom-call | tf_op jit(solution)/shard_map/stick_attention/pallas_call | solution.py:96
  64.0 2.1 convolution_convert_fusion
  66.1 0.0 all-reduce.2.cloned.1.call-update
  66.1 0.0 all-gather.11.cloned.1.call-start
  66.2 0.5 all-gather.11.cloned.1.call-update
  66.7 0.0 reduce-scatter.2.cloned.1.call-start
  66.7 45.7 %all-gather.7.cloned.1.call-done = bf16[1024,1280]{1,0:T(8,128)(2,1)} async-done(((bf16[256,1280]{1,0:T(8,128)(2,1)}), bf16[1024,1280]{1,0:T(8,128)(2,1)}) %all-gather.7.cloned.1.call-update) | async-done | bytes 2621456 | tf_op jit(solution)/shard_map/all_gather | solution.py:108
  112.5 1.5 collective-permute-start
  113.9 53.6 %all-gather.9.cloned.1.call-done = bf16[1024,1280]{1,0:T(8,128)(2,1)} async-done(((bf16[256,1280]{1,0:T(8,128)(2,1)}), bf16[1024,1280]{1,0:T(8,128)(2,1)}) %all-gather.9.cloned.1.call-update) | async-done | bytes 2621456 | tf_op jit(solution)/shard_map/all_gather | solution.py:108
  167.6 1.5 collective-permute-start.1
  169.1 50.9 %all-reduce.2.cloned.1.call-done = bf16[512,2048]{1,0:T(8,128)(2,1)} async-done(((bf16[512,2048]{1,0:T(8,128)(2,1)}), bf16[512,2048]{1,0:T(8,128)(2,1)}) %all-reduce.2.cloned.1.call-update) | async-done | bytes 2097168 | tf_op jit(solution)/shard_map/psum | solution.py:136
  220.0 2.2 fusion
  222.2 0.0 copy-done.9
  222.2 0.0 copy-done.3
  222.2 0.0 copy-start.10
  222.3 1.1 multiply_reduce_fusion
  223.4 2.0 copy-done.2
  225.4 0.0 copy-done.10
  225.4 1.8 multiply_convert_fusion
  227.2 3.4 reshape.72
  230.6 6.3 %constant_dynamic-slice_fusion.1 = (bf16[512,4,1,256]{3,2,1,0:T(2,128)(2,1)}, bf16[512,4,1,256]{3,2,1,0:T(2,128)(2,1)}) fusion(bf16[512,4,2,256]{3,2,1,0:T(2,128)(2,1)S(1)} %reshape.72, s32[]{:T(128)S(6)} %select_n.58, s32[]{:T(128)S(6)} %select_n.56), kind=kLoop, calls=%fused_computation.32 | loop fusion | bytes 4194312 | tf_op jit(solution)/shard_map/jit(dynamic_index_in_dim)/dynamic_slice | solution.py:145
  236.9 4.6 %copy.14 = bf16[512,4,1,256]{0,3,1,2:T(8,128)(2,1)S(1)} copy(bf16[512,4,1,256]{3,2,1,0:T(2,128)(2,1)} %get-tuple-element.8) | data formatting | bytes 2097152
  241.5 4.8 %copy.15 = bf16[512,4,1,256]{0,3,1,2:T(8,128)(2,1)S(1)} copy(bf16[512,4,1,256]{3,2,1,0:T(2,128)(2,1)} %get-tuple-element.7) | data formatting | bytes 2097152
  246.3 3.5 fusion.12
  249.8 3.1 fusion.13
  252.9 0.0 collective-permute-done
  252.9 4.9 %convolution_add_fusion.1 = f32[512,1280]{1,0:T(8,128)} fusion(f32[512,1280]{1,0:T(8,128)S(1)} %fusion.12, bf16[512,1024]{0,1:T(8,128)(2,1)S(1)} %bitcast.20, bf16[1024,1280]{1,0:T(8,128)(2,1)} %collective-permute-done), kind=kOutput, calls=%fused_computation.9 | convolution fusion | flops 1342832640 | bytes 8912896 | tf_op jit(solution)/shard_map/dot_general | solution.py:146
  257.8 0.0 collective-permute-done.1
  257.8 61.7 %all-gather.11.cloned.1.call-done = bf16[1280,2048]{1,0:T(8,128)(2,1)} async-done(((bf16[1280,512]{1,0:T(8,128)(2,1)}), bf16[1280,2048]{1,0:T(8,128)(2,1)}) %all-gather.11.cloned.1.call-update) | async-done | bytes 5242896 | tf_op jit(solution)/shard_map/all_gather | solution.py:134
  319.6 10.7 %convolution_convert_fusion.1 = bf16[512,2048]{1,0:T(8,128)(2,1)} fusion(bf16[1280,2048]{1,0:T(8,128)(2,1)} %all-gather.11.cloned.1.call-done, f32[512,1280]{1,0:T(8,128)} %fusion.13, bf16[512,1024]{0,1:T(8,128)(2,1)S(1)} %bitcast.21, bf16[1024,1280]{1,0:T(8,128)(2,1)} %collective-permute-done.1, f32[512,1280]{1,0:T(8,128)} %convolution_add_fusion.1), kind=kOutput, calls=%fused_computation.12 | convolution fusion | flops 4032167936 | bytes 16252928 | tf_op jit(solution)/shard_map/dot_general | solution.py:153
  330.2 0.0 reduce-scatter.2.cloned.1.call-update
  330.3 29.6 %reduce-scatter.2.cloned.1.call-done = bf16[128,2048]{1,0:T(8,128)(2,1)} async-done(((bf16[512,2048]{1,0:T(8,128)(2,1)}), bf16[128,2048]{1,0:T(8,128)(2,1)}) %reduce-scatter.2.cloned.1.call-update) | async-done | bytes 524304 | tf_op jit(solution)/shard_map/reduce_scatter | solution.py:158
  359.9 1.2 fusion.5
  361.2 2.4 fusion.9
  (22 shorter events, 0.1 us)
Async XLA Ops:
  6.5 2.1 copy-start
  6.5 3.1 copy-start.7
  6.5 4.1 %copy-start.8 = (bf16[512,256]{1,0:T(8,128)(2,1)S(1)}, bf16[512,256]{1,0:T(8,128)(2,1)}, u32[]{:S(2)}) copy-start(bf16[512,256]{1,0:T(8,128)(2,1)} %param.11) | copy-start | bytes 786436
  6.5 50.8 %all-gather.5.cloned.1.call-start = ((), (), s32[]{:S(2)}) async-start(), calls=%async_computation.1 | async-start | bytes 2621440 | tf_op jit(solution)/shard_map/all_gather | solution.py:131
  8.6 103.9 %all-gather.7.cloned.1.call-start = ((), (), s32[]{:S(2)}) async-start(), calls=%async_computation.3 | async-start | bytes 3276800 | tf_op jit(solution)/shard_map/all_gather | solution.py:108
  9.5 158.0 %all-gather.9.cloned.1.call-start = ((), (), s32[]{:S(2)}) async-start(), calls=%async_computation.4 | async-start | bytes 3276800 | tf_op jit(solution)/shard_map/all_gather | solution.py:108
  10.5 209.5 %all-reduce.2.cloned.1.call-start = ((), (), s32[]{:S(2)}) async-start(), calls=%async_computation.2 | async-start | bytes 4194304 | tf_op jit(solution)/shard_map/psum | solution.py:136
  10.7 53.3 %copy-start.6 = (bf16[256,2048]{1,0:T(8,128)(2,1)S(1)}, bf16[256,2048]{1,0:T(8,128)(2,1)}, u32[]{:S(2)}) copy-start(bf16[256,2048]{1,0:T(8,128)(2,1)} %param.15) | copy-start | bytes 3145732
  57.3 1.6 copy-start.1
  66.1 156.1 %copy-start.5 = (bf16[512,2048]{1,0:T(8,128)(2,1)S(1)}, bf16[512,2048]{1,0:T(8,128)(2,1)}, u32[]{:S(2)}) copy-start(bf16[512,2048]{1,0:T(8,128)(2,1)} %param.14) | copy-start | bytes 6291460
  66.1 156.1 %copy-start.9 = (f32[2048]{0:T(1024)S(1)}, f32[2048]{0:T(1024)}, u32[]{:S(2)}) copy-start(f32[2048]{0:T(1024)} %param.16) | copy-start | bytes 24580
  66.1 253.4 %all-gather.11.cloned.1.call-start = ((), (), s32[]{:S(2)}) async-start(), calls=%async_computation.5 | async-start | bytes 6553600 | tf_op jit(solution)/shard_map/all_gather | solution.py:134
  66.7 293.2 %reduce-scatter.2.cloned.1.call-start = ((), (), s32[]{:S(2)}) async-start(), calls=%async_computation.6 | async-start | bytes 2621440 | tf_op jit(solution)/shard_map/reduce_scatter | solution.py:158
  112.5 140.4 %collective-permute-start = (bf16[1024,1280]{1,0:T(8,128)(2,1)}, bf16[1024,1280]{1,0:T(8,128)(2,1)}, u32[]{:S(2)}, u32[]{:S(2)}) collective-permute-start(bf16[1024,1280]{1,0:T(8,128)(2,1)} %all-gather.7.cloned.1.call-done), channel_id=1, source_target_pairs={{0,16},{16,0},{1,17},{17,1},{2,18},{18,2},{3,19},{19,3},{4,20},{20... | collective-permute-start | bytes 7864328 | tf_op jit(solution)/shard_map/ppermute | solution.py:109
  167.6 90.2 %collective-permute-start.1 = (bf16[1024,1280]{1,0:T(8,128)(2,1)}, bf16[1024,1280]{1,0:T(8,128)(2,1)}, u32[]{:S(2)}, u32[]{:S(2)}) collective-permute-start(bf16[1024,1280]{1,0:T(8,128)(2,1)} %all-gather.9.cloned.1.call-done), channel_id=1, source_target_pairs={{0,16},{16,0},{1,17},{17,1},{2,18},{18,2},{3,19},{19,3},{4,20},{20... | collective-permute-start | bytes 7864328 | tf_op jit(solution)/shard_map/ppermute | solution.py:109
  220.0 2.3 copy-start.3
  222.2 3.2 copy-start.10
  223.4 2.0 copy-start.2
  246.3 3.5 copy-start.4
  330.2 30.9 %copy-start.11 = (f32[2048]{0:T(1024)S(1)}, f32[2048]{0:T(1024)}, u32[]{:S(2)}) copy-start(f32[2048]{0:T(1024)} %param.21) | copy-start | bytes 24580
Sparse Core Ops, SparseCore 0:
  8.9 48.3 all-gather.4
  58.9 53.5 all-gather.6
  114.0 53.4 all-gather.8
  169.8 50.1 all-reduce.1
  221.4 98.1 all-gather.10
  330.4 29.4 reduce-scatter.1
where the time goes:
time: 371 us; the launch traced here: 370 us
  waiting for transfers between devices  289 us (78%)
  local copies, waits for them, and re-layouts  24.5 us (7%)
  matrix products  24.3 us (7%)
  between operations  13.7 us (4%)
  other arithmetic  10.9 us (3%)
  Pallas kernels  5.03 us (1%)
    all_gather x2, waiting for transfers between devices, half_gather(): mine = lax.all_gather(mine, 'sp', axis=0, tiled=True)  99.4 us
    all_gather x1, waiting for transfers between devices, per_device(): down_all = lax.all_gather(down_weight, 'sp', axis=1, tiled=True)  61.7 us
    psum x1, waiting for transfers between devices, per_device(): lax.psum(jnp.dot(attended, out_weight, preferred_element_type=jnp.float32...  50.9 us
    all_gather x1, waiting for transfers between devices, per_device(): lax.all_gather(jnp.concatenate([keys, values], axis=1), 'sp', axis=0, til...  46.6 us
    reduce_scatter x1, waiting for transfers between devices, per_device(): lax.psum_scatter(ffn_terms.astype(jnp.bfloat16), 'tp', scatter_dimension=...  29.6 us
    unnamed x26, local copies, waits for them, and re-layouts  13 us
    dot_general x1, matrix products, per_device(): ffn_terms = jnp.dot(hidden, down_all, preferred_element_type=jnp.float32)  10.7 us
  transfers between devices with their start and end apart: 8, of which 6 were waited for; matrix products, arithmetic and copies ran while one was open for 11% of the time, Pallas kernels for 1%

commit v1 on v0

--- a/solution.py
+++ b/solution.py
@@ -102,6 +102,11 @@
     )(jnp.reshape(first_row, (1,)).astype(jnp.int32), split_queries, keys_values, keys_values)
 
 
+def trade(block, k):
+    count = lax.axis_size("tp")
+    return lax.ppermute(block, "tp", [(i, i ^ k) for i in range(count)])
+
+
 def half_gather(weight, side):
     half = weight.shape[0] // 2
     mine = lax.dynamic_slice_in_dim(weight, side * half, half, 0)
@@ -133,12 +138,19 @@
     up_mine, up_other = half_gather(up_weight, side)
     down_all = lax.all_gather(down_weight, "sp", axis=1, tiled=True)
     attended = stick_attention(queries, keys_values, lax.axis_index("sp") * tok_rows)
-    mixed_sum = lax.psum(
-        jnp.dot(attended, out_weight, preferred_element_type=jnp.float32).astype(jnp.bfloat16), "tp"
-    ).astype(jnp.float32)
-    first_all = residual.astype(jnp.float32) + rms_scale(mixed_sum, post_gain)
-    ffn_in = rms_scale(first_all, ffn_pre_gain).astype(jnp.bfloat16)
-    first_mine = lax.dynamic_slice_in_dim(first_all, my_rows, part_rows, 0)
+    parts = jnp.dot(attended, out_weight, preferred_element_type=jnp.float32).astype(jnp.bfloat16)
+    parts = parts.reshape(tp_share, part_rows, -1)
+    me = lax.axis_index("tp")
+    mixed_mine = lax.dynamic_index_in_dim(parts, me, 0, False).astype(jnp.float32)
+    for k in range(1, tp_share):
+        sent = lax.dynamic_index_in_dim(parts, jnp.bitwise_xor(me, k), 0, False)
+        mixed_mine = mixed_mine + trade(sent, k).astype(jnp.float32)
+    residual_mine = lax.dynamic_slice_in_dim(residual, my_rows, part_rows, 0)
+    first_mine = residual_mine.astype(jnp.float32) + rms_scale(mixed_mine, post_gain)
+    in_rows = rms_scale(first_mine, ffn_pre_gain).astype(jnp.bfloat16)
+    ffn_in = jnp.concatenate(
+        [in_rows] + [trade(in_rows, k) for k in range(1, tp_share)], axis=0
+    )
     half = gate_weight.shape[0] // 2
     pieces = ffn_in.reshape(tok_rows, -1, 2, half)
     in_mine = lax.dynamic_index_in_dim(pieces, side, 2, False).reshape(tok_rows, -1)
@@ -150,14 +162,19 @@
         in_other, up_other, preferred_element_type=jnp.float32
     )
     hidden = (jax.nn.silu(gate_sum) * up_sum).astype(jnp.bfloat16)
-    ffn_terms = jnp.dot(
-        hidden,
-        down_all,
-        preferred_element_type=jnp.float32,
-    )
-    ffn_out = lax.psum_scatter(
-        ffn_terms.astype(jnp.bfloat16), "tp", scatter_dimension=0, tiled=True
-    ).astype(jnp.float32)
+    near_rows = tok_rows // 2
+    far_terms = jnp.dot(
+        hidden[near_rows:], down_all, preferred_element_type=jnp.float32
+    ).astype(jnp.bfloat16)
+    near_terms = jnp.dot(
+        hidden[:near_rows], down_all, preferred_element_type=jnp.float32
+    ).astype(jnp.bfloat16)
+    blocks = [
+        near_terms[k * part_rows : (k + 1) * part_rows] for k in range(tp_share // 2)
+    ] + [far_terms[k * part_rows : (k + 1) * part_rows] for k in range(tp_share // 2)]
+    ffn_out = blocks[0].astype(jnp.float32)
+    for k in range(tp_share - 1, 0, -1):
+        ffn_out = ffn_out + trade(blocks[k], k).astype(jnp.float32)
     result = first_mine + 0.5 * rms_scale(ffn_out, ffn_post_gain)
     return result.astype(jnp.bfloat16)
 

time: 371 us -> 305 us (0.82)
  waiting for transfers between devices: 289 us -> 222 us
  starting transfers between devices: 3.15 us -> 8.85 us
  matrix products: 24.3 us -> 19.9 us
    psum x1 -> x0, waiting for transfers between devices: 50.9 us -> none  [per_device(): lax.psum(jnp.dot(attended, out_weight, preferred_element_type=jnp.float32...]
    ppermute x0 -> x9, waiting for transfers between devices: none -> 45.4 us  [trade(): return lax.ppermute(block, 'tp', [(i, i ^ k) for i in range(count)])]
    all_gather x2, waiting for transfers between devices: 99.4 us -> 66.8 us  [half_gather(): mine = lax.all_gather(mine, 'sp', axis=0, tiled=True)]
    reduce_scatter x1 -> x0, waiting for transfers between devices: 29.6 us -> none  [per_device(): lax.psum_scatter(ffn_terms.astype(jnp.bfloat16), 'tp', scatter_dimension=...]
    ppermute x2, waiting for transfers between devices: 0.01 us -> 29.4 us  [half_gather(): other = lax.ppermute(mine, 'grp', [(0, 1), (1, 0)])]
    all_gather x1, waiting for transfers between devices: 61.7 us -> 33.7 us  [per_device(): down_all = lax.all_gather(down_weight, 'sp', axis=1, tiled=True)]
    ppermute x0 -> x9, starting transfers between devices: none -> 5.77 us  [trade(): return lax.ppermute(block, 'tp', [(i, i ^ k) for i in range(count)])]
    dot_general x1 -> x3, matrix products: 10.7 us -> 10.7 us  [the longest x1 4.79 us: per_device(): jnp.dot(in_other, up_other, preferred_element_type=jnp.float32)]
  transfers between devices with their start and end apart: 8 -> 15, of which waited for: 6 -> 10; matrix products, arithmetic and copies ran while one was open for 11% -> 15% of each run, Pallas kernels for 1% -> 2%
where the time goes in v1:
time: 305 us; the launch traced here: 304 us
  waiting for transfers between devices  222 us (73%)
  local copies, waits for them, and re-layouts  23.7 us (8%)
  matrix products  19.9 us (7%)
  between operations  13.4 us (4%)
  other arithmetic  11.4 us (4%)
  starting transfers between devices  8.85 us (3%)
  Pallas kernels  5.03 us (2%)
    all_gather x2, waiting for transfers between devices, half_gather(): mine = lax.all_gather(mine, 'sp', axis=0, tiled=True)  66.8 us
    all_gather x1, waiting for transfers between devices, per_device(): lax.all_gather(jnp.concatenate([keys, values], axis=1), 'sp', axis=0, til...  46 us
    ppermute x9, waiting for transfers between devices, trade(): return lax.ppermute(block, 'tp', [(i, i ^ k) for i in range(count)])  45.4 us
    all_gather x1, waiting for transfers between devices, per_device(): down_all = lax.all_gather(down_weight, 'sp', axis=1, tiled=True)  33.7 us
    ppermute x2, waiting for transfers between devices, half_gather(): other = lax.ppermute(mine, 'grp', [(0, 1), (1, 0)])  29.4 us
    unnamed x26, local copies, waits for them, and re-layouts  11 us
    dynamic_slice x1, local copies, waits for them, and re-layouts, per_device(): lax.dynamic_index_in_dim(pieces, 1 - side, 2, False).reshape(tok_rows, -1)  6.32 us
  transfers between devices with their start and end apart: 15, of which 10 were waited for; matrix products, arithmetic and copies ran while one was open for 15% of the time, Pallas kernels for 2%

profile of v1, /device:TPU:0, one launch (start us, length us, event | category | flops | bytes accessed | tf_op | source)
XLA Modules:
  0.0 304.1 jit_solution(8667160781062932749)
XLA Ops:
  6.5 2.0 pad_maximum_fusion.2
  8.6 0.0 all-gather.7.cloned.1.call-start
  8.7 0.9 constant_dynamic-slice_fusion.2
  9.6 0.0 all-gather.9.cloned.1.call-start
  9.7 0.9 constant_dynamic-slice_fusion
  10.6 0.5 all-gather.11.cloned.1.call-update
  11.3 0.1 pad_maximum_fusion.1.q_ref
  11.3 46.0 %all-gather.5.cloned.1.call-done.k_ref.v_ref = bf16[2048,512]{1,0:T(8,128)(2,1)} async-done(((bf16[512,512]{1,0:T(8,128)(2,1)}), bf16[2048,512]{1,0:T(8,128)(2,1)}) %all-gather.5.cloned.1.call-update) | async-done | bytes 2097168 | tf_op jit(solution)/shard_map/all_gather | solution.py:136
  57.3 1.6 copy-done.1
  58.9 5.0 %stick_attention.1 = bf16[512,256]{1,0:T(8,128)(2,1)S(1)} custom-call(s32[1]{0:T(128)} %bitcast.row_ref, bf16[2,512,256]{2,1,0:T(8,128)(2,1)S(1)} %pad_maximum_fusion.1.q_ref, bf16[2048,512]{1,0:T(8,128)(2,1)S(1)} %copy-done.1, bf16[2048,512]{1,0:T(8,128)(2,1)S(1)} %copy-done.1), custom_call_target="tpu_custom_call" | custom-call | tf_op jit(solution)/shard_map/stick_attention/pallas_call | solution.py:96
  64.0 0.7 convolution_convert_fusion
  64.7 1.2 dynamic-slice_bitcast_fusion.2
  65.9 1.5 collective-permute-start.1
  67.4 0.4 collective-permute-start.2
  67.8 0.4 collective-permute-done
  68.1 12.9 %collective-permute-done.1 = bf16[128,2048]{1,0:T(8,128)(2,1)} collective-permute-done((bf16[128,2048]{1,0:T(8,128)(2,1)}, bf16[128,2048]{1,0:T(8,128)(2,1)}, u32[]{:S(2)}, u32[]{:S(2)}) %collective-permute-start.1) | collective-permute-done | bytes 524320 | tf_op jit(solution)/shard_map/ppermute | solution.py:107
  81.0 10.3 %collective-permute-done.2 = bf16[128,2048]{1,0:T(8,128)(2,1)} collective-permute-done((bf16[128,2048]{1,0:T(8,128)(2,1)}, bf16[128,2048]{1,0:T(8,128)(2,1)}, u32[]{:S(2)}, u32[]{:S(2)}) %collective-permute-start.2) | collective-permute-done | bytes 524320 | tf_op jit(solution)/shard_map/ppermute | solution.py:107
  91.3 1.7 multiply_reduce_fusion.2
  93.1 3.0 multiply_reduce_fusion.1
  96.0 16.4 %all-gather.7.cloned.1.call-done = bf16[1024,1280]{1,0:T(8,128)(2,1)} async-done(((bf16[256,1280]{1,0:T(8,128)(2,1)}), bf16[1024,1280]{1,0:T(8,128)(2,1)}) %all-gather.7.cloned.1.call-update) | async-done | bytes 2621456 | tf_op jit(solution)/shard_map/all_gather | solution.py:113
  112.5 1.5 collective-permute-start.6
  114.0 1.4 multiply_convert_fusion
  115.3 0.1 collective-permute-start.3
  115.4 1.5 collective-permute-start.4
  117.0 0.3 collective-permute-start.5
  117.3 50.3 %all-gather.9.cloned.1.call-done = bf16[1024,1280]{1,0:T(8,128)(2,1)} async-done(((bf16[256,1280]{1,0:T(8,128)(2,1)}), bf16[1024,1280]{1,0:T(8,128)(2,1)}) %all-gather.9.cloned.1.call-update) | async-done | bytes 2621456 | tf_op jit(solution)/shard_map/all_gather | solution.py:113
  167.6 1.5 collective-permute-start.7
  169.1 1.5 pad_maximum_fusion
  170.5 3.3 %reshape.78 = bf16[512,4,2,256]{3,2,1,0:T(2,128)(2,1)S(1)} reshape(bf16[512,2048]{1,0:T(8,128)(2,1)} %pad_maximum_fusion) | data formatting | bytes 4194304 | tf_op jit(solution)/shard_map/reshape | solution.py:155
  173.8 6.3 %constant_dynamic-slice_fusion.1 = (bf16[512,4,1,256]{3,2,1,0:T(2,128)(2,1)}, bf16[512,4,1,256]{3,2,1,0:T(2,128)(2,1)}) fusion(bf16[512,4,2,256]{3,2,1,0:T(2,128)(2,1)S(1)} %reshape.78, s32[]{:T(128)S(6)} %select_n.75, s32[]{:T(128)S(6)} %select_n.73), kind=kLoop, calls=%fused_computation.28 | loop fusion | bytes 4194312 | tf_op jit(solution)/shard_map/jit(dynamic_index_in_dim)/dynamic_slice | solution.py:157
  180.2 4.6 %copy.14 = bf16[512,4,1,256]{0,3,1,2:T(8,128)(2,1)S(1)} copy(bf16[512,4,1,256]{3,2,1,0:T(2,128)(2,1)} %get-tuple-element.8) | data formatting | bytes 2097152
  184.7 4.7 %copy.15 = bf16[512,4,1,256]{0,3,1,2:T(8,128)(2,1)S(1)} copy(bf16[512,4,1,256]{3,2,1,0:T(2,128)(2,1)} %get-tuple-element.7) | data formatting | bytes 2097152
  189.5 3.5 %fusion.7 = f32[512,1280]{1,0:T(8,128)S(1)} fusion(bf16[512,1024]{0,1:T(8,128)(2,1)S(1)} %bitcast.37, bf16[1024,1280]{1,0:T(8,128)(2,1)} %all-gather.7.cloned.1.call-done), kind=kOutput, calls=%fused_computation.42 | convolution fusion | flops 1342177280 | bytes 6291456 | tf_op jit(solution)/shard_map/dot_general | solution.py:158
  193.0 1.6 fusion.8
  194.6 3.3 %convolution_add_fusion.1 = f32[512,1280]{1,0:T(8,128)S(1)} fusion(f32[512,1280]{1,0:T(8,128)S(1)} %fusion.7, bf16[512,1024]{0,1:T(8,128)(2,1)S(1)} %bitcast.39, bf16[1024,1280]{1,0:T(8,128)(2,1)} %collective-permute-done.6), kind=kOutput, calls=%fused_computation.2 | convolution fusion | flops 1342832640 | bytes 8912896 | tf_op jit(solution)/shard_map/dot_general | solution.py:158
  197.9 29.4 %collective-permute-done.7 = bf16[1024,1280]{1,0:T(8,128)(2,1)} collective-permute-done((bf16[1024,1280]{1,0:T(8,128)(2,1)}, bf16[1024,1280]{1,0:T(8,128)(2,1)}, u32[]{:S(2)}, u32[]{:S(2)}) %collective-permute-start.7) | collective-permute-done | bytes 2621472 | tf_op jit(solution)/shard_map/ppermute | solution.py:114
  227.4 4.8 %fusion.1 = bf16[512,1280]{1,0:T(8,128)(2,1)} fusion(f32[512,1280]{1,0:T(8,128)S(1)} %fusion.8, bf16[512,1024]{0,1:T(8,128)(2,1)S(1)} %bitcast.40, bf16[1024,1280]{1,0:T(8,128)(2,1)} %collective-permute-done.7, f32[512,1280]{1,0:T(8,128)S(1)} %convolution_add_fusion.1), kind=kOutput, calls=%fused_computation.3 | convolution fusion | flops 1346764800 | bytes 10223616 | tf_op jit(solution)/shard_map/dot_general | solution.py:161
  232.2 33.7 %all-gather.11.cloned.1.call-done = bf16[1280,2048]{1,0:T(8,128)(2,1)} async-done(((bf16[1280,512]{1,0:T(8,128)(2,1)}), bf16[1280,2048]{1,0:T(8,128)(2,1)}) %all-gather.11.cloned.1.call-update) | async-done | bytes 5242896 | tf_op jit(solution)/shard_map/all_gather | solution.py:139
  265.9 4.4 %convolution_convert_fusion.1 = bf16[256,2048]{1,0:T(8,128)(2,1)S(1)} fusion(bf16[1280,2048]{1,0:T(8,128)(2,1)} %all-gather.11.cloned.1.call-done, bf16[512,1280]{1,0:T(8,128)(2,1)} %fusion.1), kind=kOutput, calls=%fused_computation.5 | convolution fusion | flops 1342701568 | bytes 6946816 | tf_op jit(solution)/shard_map/dot_general | solution.py:166
  270.2 0.1 fusion.6
  270.3 1.0 collective-permute-start.8
  271.3 0.6 collective-permute-start.9
  271.9 1.6 convolution_convert_fusion.2
  273.6 0.4 collective-permute-start.10
  274.0 10.6 %collective-permute-done.8 = bf16[128,2048]{1,0:T(8,128)(2,1)S(1)} collective-permute-done((bf16[128,2048]{1,0:T(8,128)(2,1)S(1)}, bf16[128,2048]{1,0:T(8,128)(2,1)S(1)}, u32[]{:S(2)}, u32[]{:S(2)}) %collective-permute-start.8) | collective-permute-done | bytes 524320 | tf_op jit(solution)/shard_map/ppermute | solution.py:107
  284.6 11.3 %collective-permute-done.9 = bf16[128,2048]{1,0:T(8,128)(2,1)S(1)} collective-permute-done((bf16[128,2048]{1,0:T(8,128)(2,1)S(1)}, bf16[128,2048]{1,0:T(8,128)(2,1)S(1)}, u32[]{:S(2)}, u32[]{:S(2)}) %collective-permute-start.9) | collective-permute-done | bytes 524320 | tf_op jit(solution)/shard_map/ppermute | solution.py:107
  295.9 0.4 multiply_reduce_fusion
  296.3 1.3 add_convert_fusion
  (40 shorter events, 0.3 us)
Async XLA Ops:
  6.5 2.1 copy-start
  6.5 3.1 %copy-start.5 = (bf16[512,1280]{1,0:T(8,128)(2,1)S(1)}, bf16[512,1280]{1,0:T(8,128)(2,1)}, u32[]{:S(2)}) copy-start(bf16[512,1280]{1,0:T(8,128)(2,1)} %param.18) | copy-start | bytes 3932164
  6.5 50.8 %all-gather.5.cloned.1.call-start = ((), (), s32[]{:S(2)}) async-start(), calls=%async_computation | async-start | bytes 2621440 | tf_op jit(solution)/shard_map/all_gather | solution.py:136
  8.6 103.9 %all-gather.7.cloned.1.call-start = ((), (), s32[]{:S(2)}) async-start(), calls=%async_computation.1 | async-start | bytes 3276800 | tf_op jit(solution)/shard_map/all_gather | solution.py:113
  8.6 2.6 copy-start.6
  9.6 158.0 %all-gather.9.cloned.1.call-start = ((), (), s32[]{:S(2)}) async-start(), calls=%async_computation.2 | async-start | bytes 3276800 | tf_op jit(solution)/shard_map/all_gather | solution.py:113
  10.6 255.3 %all-gather.11.cloned.1.call-start = ((), (), s32[]{:S(2)}) async-start(), calls=%async_computation.3 | async-start | bytes 6553600 | tf_op jit(solution)/shard_map/all_gather | solution.py:139
  57.3 1.6 copy-start.1
  58.9 5.0 %copy-start.4 = (bf16[256,2048]{1,0:T(8,128)(2,1)S(1)}, bf16[256,2048]{1,0:T(8,128)(2,1)}, u32[]{:S(2)}) copy-start(bf16[256,2048]{1,0:T(8,128)(2,1)} %param.15) | copy-start | bytes 3145732
  64.7 28.4 %copy-start.7 = (f32[2048]{0:T(1024)S(1)}, f32[2048]{0:T(1024)}, u32[]{:S(2)}) copy-start(f32[2048]{0:T(1024)} %param.16) | copy-start | bytes 24580
  65.9 2.3 collective-permute-start
  65.9 15.1 %collective-permute-start.1 = (bf16[128,2048]{1,0:T(8,128)(2,1)}, bf16[128,2048]{1,0:T(8,128)(2,1)}, u32[]{:S(2)}, u32[]{:S(2)}) collective-permute-start(bf16[128,2048]{1,0:T(8,128)(2,1)} %get-tuple-element.11), channel_id=1, source_target_pairs={{0,2},{1,3},{2,0},{3,1},{4,6},{5,7},{6,4},{7,5},{8,10},{9,11},{10,... | collective-permute-start | bytes 1572872 | tf_op jit(solution)/shard_map/ppermute | solution.py:107
  67.4 24.0 %collective-permute-start.2 = (bf16[128,2048]{1,0:T(8,128)(2,1)}, bf16[128,2048]{1,0:T(8,128)(2,1)}, u32[]{:S(2)}, u32[]{:S(2)}) collective-permute-start(bf16[128,2048]{1,0:T(8,128)(2,1)} %get-tuple-element.10), channel_id=1, source_target_pairs={{0,3},{1,2},{2,1},{3,0},{4,7},{5,6},{6,5},{7,4},{8,11},{9,10},{10,... | collective-permute-start | bytes 1572872 | tf_op jit(solution)/shard_map/ppermute | solution.py:107
  67.8 46.2 %copy-start.8 = (f32[2048]{0:T(1024)S(1)}, f32[2048]{0:T(1024)}, u32[]{:S(2)}) copy-start(f32[2048]{0:T(1024)} %param.20) | copy-start | bytes 24580
  112.5 82.1 %collective-permute-start.6 = (bf16[1024,1280]{1,0:T(8,128)(2,1)}, bf16[1024,1280]{1,0:T(8,128)(2,1)}, u32[]{:S(2)}, u32[]{:S(2)}) collective-permute-start(bf16[1024,1280]{1,0:T(8,128)(2,1)} %all-gather.7.cloned.1.call-done), channel_id=1, source_target_pairs={{0,16},{16,0},{1,17},{17,1},{2,18},{18,2},{3,19},{19,3},{4,20},{20... | collective-permute-start | bytes 7864328 | tf_op jit(solution)/shard_map/ppermute | solution.py:114
  115.3 53.7 %collective-permute-start.3 = (bf16[128,2048]{1,0:T(8,128)(2,1)S(1)}, bf16[128,2048]{1,0:T(8,128)(2,1)S(1)}, u32[]{:S(2)}, u32[]{:S(2)}) collective-permute-start(bf16[128,2048]{1,0:T(8,128)(2,1)S(1)} %multiply_convert_fusion), channel_id=1, source_target_pairs={{0,1},{1,0},{2,3},{3,2},{4,5},{5,4},{6,7},{7,6},{8,9},{9,8},{10,11... | collective-permute-start | bytes 1572872 | tf_op jit(solution)/shard_map/ppermute | solution.py:107
  115.4 53.6 %collective-permute-start.4 = (bf16[128,2048]{1,0:T(8,128)(2,1)S(1)}, bf16[128,2048]{1,0:T(8,128)(2,1)S(1)}, u32[]{:S(2)}, u32[]{:S(2)}) collective-permute-start(bf16[128,2048]{1,0:T(8,128)(2,1)S(1)} %multiply_convert_fusion), channel_id=1, source_target_pairs={{0,2},{1,3},{2,0},{3,1},{4,6},{5,7},{6,4},{7,5},{8,10},{9,11},{10,... | collective-permute-start | bytes 1572872 | tf_op jit(solution)/shard_map/ppermute | solution.py:107
  117.0 52.1 %collective-permute-start.5 = (bf16[128,2048]{1,0:T(8,128)(2,1)S(1)}, bf16[128,2048]{1,0:T(8,128)(2,1)S(1)}, u32[]{:S(2)}, u32[]{:S(2)}) collective-permute-start(bf16[128,2048]{1,0:T(8,128)(2,1)S(1)} %multiply_convert_fusion), channel_id=1, source_target_pairs={{0,3},{1,2},{2,1},{3,0},{4,7},{5,6},{6,5},{7,4},{8,11},{9,10},{10,... | collective-permute-start | bytes 1572872 | tf_op jit(solution)/shard_map/ppermute | solution.py:107
  167.6 59.8 %collective-permute-start.7 = (bf16[1024,1280]{1,0:T(8,128)(2,1)}, bf16[1024,1280]{1,0:T(8,128)(2,1)}, u32[]{:S(2)}, u32[]{:S(2)}) collective-permute-start(bf16[1024,1280]{1,0:T(8,128)(2,1)} %all-gather.9.cloned.1.call-done), channel_id=1, source_target_pairs={{0,16},{16,0},{1,17},{17,1},{2,18},{18,2},{3,19},{19,3},{4,20},{20... | collective-permute-start | bytes 7864328 | tf_op jit(solution)/shard_map/ppermute | solution.py:114
  189.5 3.5 %copy-start.3 = (bf16[1024,1280]{1,0:T(8,128)(2,1)S(1)}, bf16[1024,1280]{1,0:T(8,128)(2,1)}, u32[]{:S(2)}) copy-start(bf16[1024,1280]{1,0:T(8,128)(2,1)} %all-gather.9.cloned.1.call-done) | copy-start | bytes 7864324
  232.2 39.8 %copy-start.11 = (bf16[512,1280]{1,0:T(8,128)(2,1)S(1)}, bf16[512,1280]{1,0:T(8,128)(2,1)}, u32[]{:S(2)}) copy-start(bf16[512,1280]{1,0:T(8,128)(2,1)} %fusion.1) | copy-start | bytes 3932164
  265.9 6.1 %copy-start.10 = (bf16[1280,2048]{1,0:T(8,128)(2,1)S(1)}, bf16[1280,2048]{1,0:T(8,128)(2,1)}, u32[]{:S(2)}) copy-start(bf16[1280,2048]{1,0:T(8,128)(2,1)} %all-gather.11.cloned.1.call-done) | copy-start | bytes 15728644
  270.3 14.3 %collective-permute-start.8 = (bf16[128,2048]{1,0:T(8,128)(2,1)S(1)}, bf16[128,2048]{1,0:T(8,128)(2,1)S(1)}, u32[]{:S(2)}, u32[]{:S(2)}) collective-permute-start(bf16[128,2048]{1,0:T(8,128)(2,1)S(1)} %get-tuple-element.12), channel_id=1, source_target_pairs={{0,3},{1,2},{2,1},{3,0},{4,7},{5,6},{6,5},{7,4},{8,11},{9,10},{10,... | collective-permute-start | bytes 1572872 | tf_op jit(solution)/shard_map/ppermute | solution.py:107
  271.3 24.5 %collective-permute-start.9 = (bf16[128,2048]{1,0:T(8,128)(2,1)S(1)}, bf16[128,2048]{1,0:T(8,128)(2,1)S(1)}, u32[]{:S(2)}, u32[]{:S(2)}) collective-permute-start(bf16[128,2048]{1,0:T(8,128)(2,1)S(1)} %get-tuple-element.13), channel_id=1, source_target_pairs={{0,2},{1,3},{2,0},{3,1},{4,6},{5,7},{6,4},{7,5},{8,10},{9,11},{10,... | collective-permute-start | bytes 1572872 | tf_op jit(solution)/shard_map/ppermute | solution.py:107
  273.5 22.8 %copy-start.2 = (f32[128,2048]{1,0:T(8,128)S(1)}, f32[128,2048]{1,0:T(8,128)}, u32[]{:S(2)}) copy-start(f32[128,2048]{1,0:T(8,128)} %get-tuple-element.6) | copy-start | bytes 3145732
  273.6 22.8 %copy-start.9 = (f32[2048]{0:T(1024)S(1)}, f32[2048]{0:T(1024)}, u32[]{:S(2)}) copy-start(f32[2048]{0:T(1024)} %param.21) | copy-start | bytes 24580
  273.6 22.2 %collective-permute-start.10 = (bf16[128,2048]{1,0:T(8,128)(2,1)S(1)}, bf16[128,2048]{1,0:T(8,128)(2,1)S(1)}, u32[]{:S(2)}, u32[]{:S(2)}) collective-permute-start(bf16[128,2048]{1,0:T(8,128)(2,1)S(1)} %slice.29), channel_id=1, source_target_pairs={{0,1},{1,0},{2,3},{3,2},{4,5},{5,4},{6,7},{7,6},{8,9},{9,8},{10,11... | collective-permute-start | bytes 1572872 | tf_op jit(solution)/shard_map/ppermute | solution.py:107
Sparse Core Ops, SparseCore 0:
  8.9 48.3 all-gather.4
  58.9 53.5 all-gather.6
  114.0 53.4 all-gather.8
  169.0 96.7 all-gather.10

commit v2 on v1

--- a/solution.py
+++ b/solution.py
@@ -136,7 +136,19 @@
     keys_values = lax.all_gather(jnp.concatenate([keys, values], axis=1), "sp", axis=0, tiled=True)
     gate_mine, gate_other = half_gather(gate_weight, side)
     up_mine, up_other = half_gather(up_weight, side)
-    down_all = lax.all_gather(down_weight, "sp", axis=1, tiled=True)
+    swap_rows = down_weight.shape[0] // 5
+    down_mine = lax.dynamic_slice_in_dim(down_weight, side * swap_rows, swap_rows, 0)
+    down_mine = lax.all_gather(down_mine, "sp", axis=1, tiled=True)
+    down_other = lax.ppermute(down_mine, "grp", [(0, 1), (1, 0)])
+    down_top = jnp.concatenate(
+        [
+            jnp.where(side == 0, down_mine, down_other),
+            jnp.where(side == 0, down_other, down_mine),
+        ],
+        axis=0,
+    )
+    top_rows = 2 * swap_rows
+    down_rest = lax.all_gather(down_weight[top_rows:], "sp", axis=1, tiled=True)
     attended = stick_attention(queries, keys_values, lax.axis_index("sp") * tok_rows)
     parts = jnp.dot(attended, out_weight, preferred_element_type=jnp.float32).astype(jnp.bfloat16)
     parts = parts.reshape(tp_share, part_rows, -1)
@@ -163,11 +175,13 @@
     )
     hidden = (jax.nn.silu(gate_sum) * up_sum).astype(jnp.bfloat16)
     near_rows = tok_rows // 2
-    far_terms = jnp.dot(
-        hidden[near_rows:], down_all, preferred_element_type=jnp.float32
+    far_terms = (
+        jnp.dot(hidden[near_rows:, :top_rows], down_top, preferred_element_type=jnp.float32)
+        + jnp.dot(hidden[near_rows:, top_rows:], down_rest, preferred_element_type=jnp.float32)
     ).astype(jnp.bfloat16)
-    near_terms = jnp.dot(
-        hidden[:near_rows], down_all, preferred_element_type=jnp.float32
+    near_terms = (
+        jnp.dot(hidden[:near_rows, :top_rows], down_top, preferred_element_type=jnp.float32)
+        + jnp.dot(hidden[:near_rows, top_rows:], down_rest, preferred_element_type=jnp.float32)
     ).astype(jnp.bfloat16)
     blocks = [
         near_terms[k * part_rows : (k + 1) * part_rows] for k in range(tp_share // 2)

time: 305 us -> 297 us (0.974)
  waiting for transfers between devices: 222 us -> 210 us
    all_gather x2, waiting for transfers between devices: 66.8 us -> 97.8 us  [half_gather(): mine = lax.all_gather(mine, 'sp', axis=0, tiled=True)]
    ppermute x9, waiting for transfers between devices: 45.4 us -> 23 us  [trade(): return lax.ppermute(block, 'tp', [(i, i ^ k) for i in range(count)])]
    all_gather x1 -> x2, waiting for transfers between devices: 33.7 us -> 16.9 us  [the longest x1 16.9 us: per_device(): down_mine = lax.all_gather(down_mine, 'sp', axis=1, tiled=True)]
    unnamed x26 -> x44, local copies, waits for them, and re-layouts: 11 us -> 10.6 us
  transfers between devices with their start and end apart: 15 -> 17, of which waited for: 10 -> 8; matrix products, arithmetic and copies ran while one was open for 15% -> 16% of each run, Pallas kernels for 2% -> 2%
where the time goes in v2:
time: 297 us
  waiting for transfers between devices  210 us (71%)
  local copies, waits for them, and re-layouts  26.1 us (9%)
  matrix products  19.6 us (7%)
  between operations  13.6 us (5%)
  other arithmetic  12.1 us (4%)
  starting transfers between devices  10.6 us (4%)
  Pallas kernels  5.03 us (2%)
    all_gather x2, waiting for transfers between devices, half_gather(): mine = lax.all_gather(mine, 'sp', axis=0, tiled=True)  97.8 us
    all_gather x1, waiting for transfers between devices, per_device(): lax.all_gather(jnp.concatenate([keys, values], axis=1), 'sp', axis=0, til...  44.8 us
    ppermute x2, waiting for transfers between devices, half_gather(): other = lax.ppermute(mine, 'grp', [(0, 1), (1, 0)])  26.9 us
    ppermute x9, waiting for transfers between devices, trade(): return lax.ppermute(block, 'tp', [(i, i ^ k) for i in range(count)])  23 us
    all_gather x1, waiting for transfers between devices, per_device(): down_mine = lax.all_gather(down_mine, 'sp', axis=1, tiled=True)  16.9 us
    unnamed x44, local copies, waits for them, and re-layouts  10.6 us
    dynamic_slice x1, local copies, waits for them, and re-layouts, per_device(): lax.dynamic_index_in_dim(pieces, 1 - side, 2, False).reshape(tok_rows, -1)  6.31 us
    ppermute x9, starting transfers between devices, trade(): return lax.ppermute(block, 'tp', [(i, i ^ k) for i in range(count)])  6.05 us
  transfers between devices with their start and end apart: 17, of which 8 were waited for; matrix products, arithmetic and copies ran while one was open for 16% of the time, Pallas kernels for 2%

profile of v2, /device:TPU:0, one launch (start us, length us, event | category | flops | bytes accessed | tf_op | source)
XLA Modules:
  0.0 296.6 jit_solution(7289520569194385270)
XLA Ops:
  6.5 2.0 pad_maximum_fusion.5
  8.6 1.7 constant_dynamic-slice_fusion
  10.4 0.9 constant_dynamic-slice_fusion.3
  11.4 0.9 constant_dynamic-slice_fusion.1
  12.5 0.1 pad_maximum_fusion.4.q_ref
  12.5 44.8 %all-gather.6.cloned.1.call-done.k_ref.v_ref = bf16[2048,512]{1,0:T(8,128)(2,1)} async-done(((bf16[512,512]{1,0:T(8,128)(2,1)}), bf16[2048,512]{1,0:T(8,128)(2,1)}) %all-gather.6.cloned.1.call-update) | async-done | bytes 2097168 | tf_op jit(solution)/shard_map/all_gather | solution.py:136
  57.3 1.6 copy-done.2
  58.9 5.0 %stick_attention.1 = bf16[512,256]{1,0:T(8,128)(2,1)S(1)} custom-call(s32[1]{0:T(128)} %bitcast.row_ref, bf16[2,512,256]{2,1,0:T(8,128)(2,1)S(1)} %pad_maximum_fusion.4.q_ref, bf16[2048,512]{1,0:T(8,128)(2,1)S(1)} %copy-done.2, bf16[2048,512]{1,0:T(8,128)(2,1)S(1)} %copy-done.2), custom_call_target="tpu_custom_call" | custom-call | tf_op jit(solution)/shard_map/stick_attention/pallas_call | solution.py:96
  64.0 0.7 convolution_convert_fusion
  64.7 1.2 dynamic-slice_bitcast_fusion.2
  65.9 1.5 collective-permute-start.1
  67.4 0.4 collective-permute-start.2
  67.8 1.0 slice.29
  68.8 16.9 %all-gather.12.cloned.1.call-done = bf16[256,2048]{1,0:T(8,128)(2,1)} async-done(((bf16[256,512]{1,0:T(8,128)(2,1)}), bf16[256,2048]{1,0:T(8,128)(2,1)}) %all-gather.12.cloned.1.call-update) | async-done | bytes 1048592 | tf_op jit(solution)/shard_map/all_gather | solution.py:141
  85.7 1.5 collective-permute-start.8
  87.2 4.1 %collective-permute-done.2 = bf16[128,2048]{1,0:T(8,128)(2,1)} collective-permute-done((bf16[128,2048]{1,0:T(8,128)(2,1)}, bf16[128,2048]{1,0:T(8,128)(2,1)}, u32[]{:S(2)}, u32[]{:S(2)}) %collective-permute-start.2) | collective-permute-done | bytes 524320 | tf_op jit(solution)/shard_map/ppermute | solution.py:107
  91.3 1.4 multiply_reduce_fusion.2
  92.8 2.2 multiply_reduce_fusion.1
  95.0 46.4 %all-gather.8.cloned.1.call-done = bf16[1024,1280]{1,0:T(8,128)(2,1)} async-done(((bf16[256,1280]{1,0:T(8,128)(2,1)}), bf16[1024,1280]{1,0:T(8,128)(2,1)}) %all-gather.8.cloned.1.call-update) | async-done | bytes 2621456 | tf_op jit(solution)/shard_map/all_gather | solution.py:113
  141.4 1.5 collective-permute-start.6
  142.9 0.2 multiply_convert_fusion
  143.1 0.1 collective-permute-start.3
  143.2 1.5 collective-permute-start.4
  144.7 0.3 collective-permute-start.5
  145.0 51.4 %all-gather.10.cloned.1.call-done = bf16[1024,1280]{1,0:T(8,128)(2,1)} async-done(((bf16[256,1280]{1,0:T(8,128)(2,1)}), bf16[1024,1280]{1,0:T(8,128)(2,1)}) %all-gather.10.cloned.1.call-update) | async-done | bytes 2621456 | tf_op jit(solution)/shard_map/all_gather | solution.py:113
  196.4 1.5 collective-permute-start.7
  197.9 3.0 %broadcast_select_fusion.1 = (bf16[256,2048]{1,0:T(8,128)(2,1)}, bf16[256,2048]{1,0:T(8,128)(2,1)}) fusion(bf16[256,2048]{1,0:T(8,128)(2,1)} %all-gather.12.cloned.1.call-done, bf16[256,2048]{1,0:T(8,128)(2,1)} %collective-permute-done.8, pred[]{:T(512)S(6)} %eq.26), kind=kLoop, calls=%fused_computation.22 | loop fusion | flops 1048576 | bytes 4194305 | tf_op jit(solution)/shard_map/jit(_where)/select_n | solution.py:145
  200.9 1.5 pad_maximum_fusion
  202.4 3.4 %reshape.78 = bf16[512,4,2,256]{3,2,1,0:T(2,128)(2,1)S(1)} reshape(bf16[512,2048]{1,0:T(8,128)(2,1)} %pad_maximum_fusion) | data formatting | bytes 4194304 | tf_op jit(solution)/shard_map/reshape | solution.py:167
  205.7 6.3 %constant_dynamic-slice_fusion.2 = (bf16[512,4,1,256]{3,2,1,0:T(2,128)(2,1)}, bf16[512,4,1,256]{3,2,1,0:T(2,128)(2,1)}) fusion(bf16[512,4,2,256]{3,2,1,0:T(2,128)(2,1)S(1)} %reshape.78, s32[]{:T(128)S(6)} %select_n.90, s32[]{:T(128)S(6)} %select_n.88), kind=kLoop, calls=%fused_computation.38 | loop fusion | bytes 4194312 | tf_op jit(solution)/shard_map/jit(dynamic_index_in_dim)/dynamic_slice | solution.py:169
  212.0 4.7 %copy.14 = bf16[512,4,1,256]{0,3,1,2:T(8,128)(2,1)S(1)} copy(bf16[512,4,1,256]{3,2,1,0:T(2,128)(2,1)} %get-tuple-element.10) | data formatting | bytes 2097152
  216.8 4.2 %copy.15 = bf16[512,4,1,256]{0,3,1,2:T(8,128)(2,1)} copy(bf16[512,4,1,256]{3,2,1,0:T(2,128)(2,1)S(1)} %copy-done.6) | data formatting | bytes 2097152
  221.0 3.5 %fusion.15 = f32[512,1280]{1,0:T(8,128)S(1)} fusion(bf16[512,1024]{0,1:T(8,128)(2,1)S(1)} %bitcast.37, bf16[1024,1280]{1,0:T(8,128)(2,1)} %all-gather.8.cloned.1.call-done), kind=kOutput, calls=%fused_computation.54 | convolution fusion | flops 1342177280 | bytes 6291456 | tf_op jit(solution)/shard_map/dot_general | solution.py:170
  224.5 1.6 fusion.16
  226.1 3.4 %convolution_add_fusion.1 = f32[512,1280]{1,0:T(8,128)S(1)} fusion(f32[512,1280]{1,0:T(8,128)S(1)} %fusion.15, bf16[512,1024]{0,1:T(8,128)(2,1)S(1)} %bitcast.39, bf16[1024,1280]{1,0:T(8,128)(2,1)} %collective-permute-done.6), kind=kOutput, calls=%fused_computation.2 | convolution fusion | flops 1342832640 | bytes 8912896 | tf_op jit(solution)/shard_map/dot_general | solution.py:170
  229.5 26.9 %collective-permute-done.7 = bf16[1024,1280]{1,0:T(8,128)(2,1)} collective-permute-done((bf16[1024,1280]{1,0:T(8,128)(2,1)}, bf16[1024,1280]{1,0:T(8,128)(2,1)}, u32[]{:S(2)}, u32[]{:S(2)}) %collective-permute-start.7) | collective-permute-done | bytes 2621472 | tf_op jit(solution)/shard_map/ppermute | solution.py:114
  256.4 4.8 %fusion.1 = bf16[512,1280]{1,0:T(8,128)(2,1)} fusion(f32[512,1280]{1,0:T(8,128)S(1)} %fusion.16, bf16[512,1024]{0,1:T(8,128)(2,1)S(1)} %bitcast.40, bf16[1024,1280]{1,0:T(8,128)(2,1)} %collective-permute-done.7, f32[512,1280]{1,0:T(8,128)S(1)} %convolution_add_fusion.1), kind=kOutput, calls=%fused_computation.3 | convolution fusion | flops 1346764800 | bytes 10223616 | tf_op jit(solution)/shard_map/dot_general | solution.py:173
  261.2 3.1 %fusion.6 = f32[256,2048]{1,0:T(8,128)S(1)} fusion(bf16[768,2048]{1,0:T(8,128)(2,1)} %all-gather.14.cloned.1.call-done, bf16[512,1280]{1,0:T(8,128)(2,1)} %fusion.1), kind=kOutput, calls=%fused_computation.28 | convolution fusion | flops 805306368 | bytes 5636096 | tf_op jit(solution)/shard_map/dot_general | solution.py:180
  264.4 0.8 fusion.3
  265.1 0.1 fusion.14
  265.2 1.5 collective-permute-start.10
  266.8 1.0 fusion.8
  267.8 0.8 fusion.2
  268.6 0.7 collective-permute-start.11
  269.4 10.8 %collective-permute-done.10 = bf16[128,2048]{1,0:T(8,128)(2,1)S(1)} collective-permute-done((bf16[128,2048]{1,0:T(8,128)(2,1)S(1)}, bf16[128,2048]{1,0:T(8,128)(2,1)S(1)}, u32[]{:S(2)}, u32[]{:S(2)}) %collective-permute-start.10) | collective-permute-done | bytes 524320 | tf_op jit(solution)/shard_map/ppermute | solution.py:107
  280.1 8.2 %collective-permute-done.9 = bf16[128,2048]{1,0:T(8,128)(2,1)S(1)} collective-permute-done((bf16[128,2048]{1,0:T(8,128)(2,1)S(1)}, bf16[128,2048]{1,0:T(8,128)(2,1)S(1)}, u32[]{:S(2)}, u32[]{:S(2)}) %collective-permute-start.9) | collective-permute-done | bytes 524320 | tf_op jit(solution)/shard_map/ppermute | solution.py:107
  288.3 0.4 multiply_reduce_fusion
  288.8 1.3 add_convert_fusion
  (68 shorter events, 0.5 us)
Async XLA Ops:
  6.5 3.9 %copy-start = (bf16[512,1280]{1,0:T(8,128)(2,1)S(1)}, bf16[512,1280]{1,0:T(8,128)(2,1)}, u32[]{:S(2)}) copy-start(bf16[512,1280]{1,0:T(8,128)(2,1)} %param.17) | copy-start | bytes 3932164
  6.5 4.9 %copy-start.16 = (bf16[512,1280]{1,0:T(8,128)(2,1)S(1)}, bf16[512,1280]{1,0:T(8,128)(2,1)}, u32[]{:S(2)}) copy-start(bf16[512,1280]{1,0:T(8,128)(2,1)} %param.18) | copy-start | bytes 3932164
  6.5 50.8 %all-gather.6.cloned.1.call-start = ((), (), s32[]{:S(2)}) async-start(), calls=%async_computation | async-start | bytes 2621440 | tf_op jit(solution)/shard_map/all_gather | solution.py:136
  8.6 3.9 %copy-start.17 = (bf16[512,256]{1,0:T(8,128)(2,1)S(1)}, bf16[512,256]{1,0:T(8,128)(2,1)}, u32[]{:S(2)}) copy-start(bf16[512,256]{1,0:T(8,128)(2,1)} %param.11) | copy-start | bytes 786436
  8.6 77.1 %all-gather.12.cloned.1.call-start = ((), (), s32[]{:S(2)}) async-start(), calls=%async_computation.3 | async-start | bytes 1310720 | tf_op jit(solution)/shard_map/all_gather | solution.py:141
  10.3 131.1 %all-gather.8.cloned.1.call-start = ((), (), s32[]{:S(2)}) async-start(), calls=%async_computation.1 | async-start | bytes 3276800 | tf_op jit(solution)/shard_map/all_gather | solution.py:113
  11.3 185.1 %all-gather.10.cloned.1.call-start = ((), (), s32[]{:S(2)}) async-start(), calls=%async_computation.2 | async-start | bytes 3276800 | tf_op jit(solution)/shard_map/all_gather | solution.py:113
  12.3 248.9 %all-gather.14.cloned.1.call-start = ((), (), s32[]{:S(2)}) async-start(), calls=%async_computation.4 | async-start | bytes 3932160 | tf_op jit(solution)/shard_map/all_gather | solution.py:151
  57.3 1.6 copy-start.2
  58.9 5.0 %copy-start.13 = (bf16[256,2048]{1,0:T(8,128)(2,1)S(1)}, bf16[256,2048]{1,0:T(8,128)(2,1)}, u32[]{:S(2)}) copy-start(bf16[256,2048]{1,0:T(8,128)(2,1)} %param.15) | copy-start | bytes 3145732
  64.0 3.8 %copy-start.14 = (bf16[1280,512]{1,0:T(8,128)(2,1)S(1)}, bf16[1280,512]{1,0:T(8,128)(2,1)}, u32[]{:S(2)}) copy-start(bf16[1280,512]{1,0:T(8,128)(2,1)} %param.19) | copy-start | bytes 3932164
  65.9 26.9 %copy-start.18 = (f32[2048]{0:T(1024)S(1)}, f32[2048]{0:T(1024)}, u32[]{:S(2)}) copy-start(f32[2048]{0:T(1024)} %param.16) | copy-start | bytes 24580
  65.9 21.3 %collective-permute-start = (bf16[128,2048]{1,0:T(8,128)(2,1)}, bf16[128,2048]{1,0:T(8,128)(2,1)S(1)}, u32[]{:S(2)}, u32[]{:S(2)}) collective-permute-start(bf16[128,2048]{1,0:T(8,128)(2,1)} %get-tuple-element.11), channel_id=1, source_target_pairs={{0,1},{1,0},{2,3},{3,2},{4,5},{5,4},{6,7},{7,6},{8,9},{9,8},{10,11... | collective-permute-start | bytes 1572872 | tf_op jit(solution)/shard_map/ppermute | solution.py:107
  65.9 21.3 %collective-permute-start.1 = (bf16[128,2048]{1,0:T(8,128)(2,1)}, bf16[128,2048]{1,0:T(8,128)(2,1)S(1)}, u32[]{:S(2)}, u32[]{:S(2)}) collective-permute-start(bf16[128,2048]{1,0:T(8,128)(2,1)} %get-tuple-element.13), channel_id=1, source_target_pairs={{0,2},{1,3},{2,0},{3,1},{4,6},{5,7},{6,4},{7,5},{8,10},{9,11},{10,... | collective-permute-start | bytes 1572872 | tf_op jit(solution)/shard_map/ppermute | solution.py:107
  67.4 24.0 %collective-permute-start.2 = (bf16[128,2048]{1,0:T(8,128)(2,1)}, bf16[128,2048]{1,0:T(8,128)(2,1)}, u32[]{:S(2)}, u32[]{:S(2)}) collective-permute-start(bf16[128,2048]{1,0:T(8,128)(2,1)} %get-tuple-element.12), channel_id=1, source_target_pairs={{0,3},{1,2},{2,1},{3,0},{4,7},{5,6},{6,5},{7,4},{8,11},{9,10},{10,... | collective-permute-start | bytes 1572872 | tf_op jit(solution)/shard_map/ppermute | solution.py:107
  68.8 74.1 %copy-start.19 = (f32[2048]{0:T(1024)S(1)}, f32[2048]{0:T(1024)}, u32[]{:S(2)}) copy-start(f32[2048]{0:T(1024)} %param.20) | copy-start | bytes 24580
  85.7 59.3 %collective-permute-start.8 = (bf16[256,2048]{1,0:T(8,128)(2,1)}, bf16[256,2048]{1,0:T(8,128)(2,1)}, u32[]{:S(2)}, u32[]{:S(2)}) collective-permute-start(bf16[256,2048]{1,0:T(8,128)(2,1)} %all-gather.12.cloned.1.call-done), channel_id=1, source_target_pairs={{0,16},{16,0},{1,17},{17,1},{2,18},{18,2},{3,19},{19,3},{4,20},{20... | collective-permute-start | bytes 3145736 | tf_op jit(solution)/shard_map/ppermute | solution.py:142
  87.2 5.6 %copy-start.9 = (bf16[128,2048]{1,0:T(8,128)(2,1)}, bf16[128,2048]{1,0:T(8,128)(2,1)S(1)}, u32[]{:S(2)}) copy-start(bf16[128,2048]{1,0:T(8,128)(2,1)S(1)} %collective-permute-done) | copy-start | bytes 1572868
  87.2 5.6 %copy-start.10 = (bf16[128,2048]{1,0:T(8,128)(2,1)}, bf16[128,2048]{1,0:T(8,128)(2,1)S(1)}, u32[]{:S(2)}) copy-start(bf16[128,2048]{1,0:T(8,128)(2,1)S(1)} %collective-permute-done.1) | copy-start | bytes 1572868
  95.0 105.9 %copy-start.4 = (f32[128,2048]{1,0:T(8,128)}, f32[128,2048]{1,0:T(8,128)S(1)}, u32[]{:S(2)}) copy-start(f32[128,2048]{1,0:T(8,128)S(1)} %get-tuple-element.6) | copy-start | bytes 3145732
  141.4 84.6 %collective-permute-start.6 = (bf16[1024,1280]{1,0:T(8,128)(2,1)}, bf16[1024,1280]{1,0:T(8,128)(2,1)}, u32[]{:S(2)}, u32[]{:S(2)}) collective-permute-start(bf16[1024,1280]{1,0:T(8,128)(2,1)} %all-gather.8.cloned.1.call-done), channel_id=1, source_target_pairs={{0,16},{16,0},{1,17},{17,1},{2,18},{18,2},{3,19},{19,3},{4,20},{20... | collective-permute-start | bytes 7864328 | tf_op jit(solution)/shard_map/ppermute | solution.py:114
  143.1 57.8 %collective-permute-start.3 = (bf16[128,2048]{1,0:T(8,128)(2,1)S(1)}, bf16[128,2048]{1,0:T(8,128)(2,1)S(1)}, u32[]{:S(2)}, u32[]{:S(2)}) collective-permute-start(bf16[128,2048]{1,0:T(8,128)(2,1)S(1)} %multiply_convert_fusion), channel_id=1, source_target_pairs={{0,1},{1,0},{2,3},{3,2},{4,5},{5,4},{6,7},{7,6},{8,9},{9,8},{10,11... | collective-permute-start | bytes 1572872 | tf_op jit(solution)/shard_map/ppermute | solution.py:107
  143.2 57.7 %collective-permute-start.4 = (bf16[128,2048]{1,0:T(8,128)(2,1)S(1)}, bf16[128,2048]{1,0:T(8,128)(2,1)S(1)}, u32[]{:S(2)}, u32[]{:S(2)}) collective-permute-start(bf16[128,2048]{1,0:T(8,128)(2,1)S(1)} %multiply_convert_fusion), channel_id=1, source_target_pairs={{0,2},{1,3},{2,0},{3,1},{4,6},{5,7},{6,4},{7,5},{8,10},{9,11},{10,... | collective-permute-start | bytes 1572872 | tf_op jit(solution)/shard_map/ppermute | solution.py:107
  144.7 56.2 %collective-permute-start.5 = (bf16[128,2048]{1,0:T(8,128)(2,1)S(1)}, bf16[128,2048]{1,0:T(8,128)(2,1)S(1)}, u32[]{:S(2)}, u32[]{:S(2)}) collective-permute-start(bf16[128,2048]{1,0:T(8,128)(2,1)S(1)} %multiply_convert_fusion), channel_id=1, source_target_pairs={{0,3},{1,2},{2,1},{3,0},{4,7},{5,6},{6,5},{7,4},{8,11},{9,10},{10,... | collective-permute-start | bytes 1572872 | tf_op jit(solution)/shard_map/ppermute | solution.py:107
  196.4 60.0 %collective-permute-start.7 = (bf16[1024,1280]{1,0:T(8,128)(2,1)}, bf16[1024,1280]{1,0:T(8,128)(2,1)}, u32[]{:S(2)}, u32[]{:S(2)}) collective-permute-start(bf16[1024,1280]{1,0:T(8,128)(2,1)} %all-gather.10.cloned.1.call-done), channel_id=1, source_target_pairs={{0,16},{16,0},{1,17},{17,1},{2,18},{18,2},{3,19},{19,3},{4,20},{20... | collective-permute-start | bytes 7864328 | tf_op jit(solution)/shard_map/ppermute | solution.py:114
  212.0 4.7 %copy-start.6 = (bf16[512,4,1,256]{3,2,1,0:T(2,128)(2,1)S(1)}, bf16[512,4,1,256]{3,2,1,0:T(2,128)(2,1)}, u32[]{:S(2)}) copy-start(bf16[512,4,1,256]{3,2,1,0:T(2,128)(2,1)} %get-tuple-element.9) | copy-start | bytes 3145732
  221.0 3.5 %copy-start.8 = (bf16[1024,1280]{1,0:T(8,128)(2,1)S(1)}, bf16[1024,1280]{1,0:T(8,128)(2,1)}, u32[]{:S(2)}) copy-start(bf16[1024,1280]{1,0:T(8,128)(2,1)} %all-gather.10.cloned.1.call-done) | copy-start | bytes 7864324
  224.5 1.6 copy-start.7
  261.2 3.2 %copy-start.11 = (bf16[256,2048]{1,0:T(8,128)(2,1)S(1)}, bf16[256,2048]{1,0:T(8,128)(2,1)}, u32[]{:S(2)}) copy-start(bf16[256,2048]{1,0:T(8,128)(2,1)} %get-tuple-element.7) | copy-start | bytes 3145732
  261.2 3.2 %copy-start.12 = (bf16[256,2048]{1,0:T(8,128)(2,1)S(1)}, bf16[256,2048]{1,0:T(8,128)(2,1)}, u32[]{:S(2)}) copy-start(bf16[256,2048]{1,0:T(8,128)(2,1)} %get-tuple-element.8) | copy-start | bytes 3145732
  261.2 3.2 %copy-start.15 = (bf16[512,1280]{1,0:T(8,128)(2,1)S(1)}, bf16[512,1280]{1,0:T(8,128)(2,1)}, u32[]{:S(2)}) copy-start(bf16[512,1280]{1,0:T(8,128)(2,1)} %fusion.1) | copy-start | bytes 3932164
  264.4 2.4 copy-start.3
  265.2 14.9 %collective-permute-start.10 = (bf16[128,2048]{1,0:T(8,128)(2,1)S(1)}, bf16[128,2048]{1,0:T(8,128)(2,1)S(1)}, u32[]{:S(2)}, u32[]{:S(2)}) collective-permute-start(bf16[128,2048]{1,0:T(8,128)(2,1)S(1)} %get-tuple-element.15), channel_id=1, source_target_pairs={{0,2},{1,3},{2,0},{3,1},{4,6},{5,7},{6,4},{7,5},{8,10},{9,11},{10,... | collective-permute-start | bytes 1572872 | tf_op jit(solution)/shard_map/ppermute | solution.py:107
  266.8 21.5 %collective-permute-start.9 = (bf16[128,2048]{1,0:T(8,128)(2,1)S(1)}, bf16[128,2048]{1,0:T(8,128)(2,1)S(1)}, u32[]{:S(2)}, u32[]{:S(2)}) collective-permute-start(bf16[128,2048]{1,0:T(8,128)(2,1)S(1)} %get-tuple-element.14), channel_id=1, source_target_pairs={{0,3},{1,2},{2,1},{3,0},{4,7},{5,6},{6,5},{7,4},{8,11},{9,10},{10,... | collective-permute-start | bytes 1572872 | tf_op jit(solution)/shard_map/ppermute | solution.py:107
  268.5 20.2 %copy-start.5 = (f32[128,2048]{1,0:T(8,128)S(1)}, f32[128,2048]{1,0:T(8,128)}, u32[]{:S(2)}) copy-start(f32[128,2048]{1,0:T(8,128)} %copy-done.4) | copy-start | bytes 3145732
  268.6 20.2 %copy-start.20 = (f32[2048]{0:T(1024)S(1)}, f32[2048]{0:T(1024)}, u32[]{:S(2)}) copy-start(f32[2048]{0:T(1024)} %param.21) | copy-start | bytes 24580
  268.6 21.5 %copy-start.1 = (bf16[512,1280]{1,0:T(8,128)(2,1)S(1)}, bf16[512,1280]{1,0:T(8,128)(2,1)}, u32[]{:S(2)}) copy-start(bf16[512,1280]{1,0:T(8,128)(2,1)} %param.17) | copy-start | bytes 3932164
  268.6 19.6 %collective-permute-start.11 = (bf16[128,2048]{1,0:T(8,128)(2,1)S(1)}, bf16[128,2048]{1,0:T(8,128)(2,1)S(1)}, u32[]{:S(2)}, u32[]{:S(2)}) collective-permute-start(bf16[128,2048]{1,0:T(8,128)(2,1)S(1)} %slice.43), channel_id=1, source_target_pairs={{0,1},{1,0},{2,3},{3,2},{4,5},{5,4},{6,7},{7,6},{8,9},{9,8},{10,11... | collective-permute-start | bytes 1572872 | tf_op jit(solution)/shard_map/ppermute | solution.py:107
Sparse Core Ops, SparseCore 0:
  8.9 48.3 all-gather.5
  58.9 26.7 all-gather.11
  87.3 54.0 all-gather.7
  142.9 53.5 all-gather.9
  197.8 62.1 all-gather.13
